TPU v7x, 32 devices: a whole 2x2x4 slice. The times are simulated.
32 devices in a mesh: sp: 8 (over z, y), tp: 4 (over x, core).
Axes of the slice: x: 2, y: 2, z: 4, core: 2. Of those that a mesh axis runs over, the one named last changes fastest.
Arguments:
- stream: bfloat16 [3072, 2048], P(('sp', 'tp')), may hold values from -6 to 6
- query_projected: bfloat16 [3072, 1024], P('sp', 'tp'), may hold values from -6 to 6
- key_projected: bfloat16 [3072, 1024], P('sp', 'tp'), may hold values from -6 to 6
- value_projected: bfloat16 [3072, 1024], P('sp', 'tp'), may hold values from -6 to 6
- gate_projected: bfloat16 [3072, 1024], P('sp', 'tp'), may hold values from -6 to 6
- strength_logits: bfloat16 [8, 3072], P('tp', 'sp'), may hold values from -7 to 4
- decay_preactivation: bfloat16 [8, 3072], P('tp', 'sp'), may hold values from -9 to 9
- extra_log_decay: float32 [8, 3072], P('tp', 'sp'), may hold values from -0.7 to 0
- head_decay_rate: float32 [8], P('tp'), may hold values from 0 to 0.1
- head_norm_gain: float32 [128], replicated, may hold values from 0.1 to 1.9
- head_output_matrix: bfloat16 [1024, 2048], P('tp'), may hold values from -0.1875 to 0.1875
- feed_norm_gain: float32 [2048], replicated, may hold values from 0.1 to 1.9
- gate_matrix: bfloat16 [2048, 5632], P('sp', 'tp'), may hold values from -0.125 to 0.125
- up_matrix: bfloat16 [2048, 5632], P('sp', 'tp'), may hold values from -0.125 to 0.125
- down_matrix: bfloat16 [5632, 2048], P('tp', 'sp'), may hold values from -0.078125 to 0.078125
Outputs:
- result: bfloat16 [3072, 2048], P(('sp', 'tp'))
All inputs are finite; a program needn't handle non-finite values.
Results may differ from a plain program's by a relative error of at most 0.015.
Values may be sent and summed in bfloat16 or wider, within the bound.
No kernel may reach another device: no remote copies, remote signals or barrier semaphores. Data moves between devices by JAX's collectives and lax.ppermute only.
A program may use at most 128 MiB of HBM per device.

v0:
```python
import jax
import jax.numpy as jnp
from jax import lax
from jax.sharding import PartitionSpec as P

HEAD = 128
BLOCK = 64
PRECISION_FULL = lax.Precision.HIGHEST
EPSILON = 1e-06


def from_behind(value, axis, by):
    size = lax.axis_size(axis)
    pairs = [(i, i + by) for i in range(size) if 0 <= i + by < size]
    return lax.ppermute(value, axis, pairs)


def unit_rows(tensor):
    return tensor * lax.rsqrt(jnp.sum(tensor * tensor, axis=-1, keepdims=True) + EPSILON)


def rms_scale(tensor):
    return tensor * lax.rsqrt(jnp.mean(tensor * tensor, axis=-1, keepdims=True) + EPSILON)


def block_correction(
    unit_queries,
    unit_keys,
    complete_values,
    strength_logits,
    decay_preactivation,
    extra_log_decay,
    head_decay_rate,
):
    head_count, length, head_width = unit_queries.shape
    block_count = length // BLOCK

    def to_blocks(tensor):
        return tensor.reshape((head_count, block_count, BLOCK) + tensor.shape[2:])

    beta_gate = jax.nn.sigmoid(strength_logits.astype(jnp.float32))
    decay_logarithm = (
        -head_decay_rate[:, None] * jax.nn.softplus(decay_preactivation.astype(jnp.float32))
        + extra_log_decay
    )
    query_block = to_blocks(unit_queries)
    key_block = to_blocks(unit_keys)
    value_block = to_blocks(complete_values)
    beta_block = to_blocks(beta_gate)
    cumulative = jnp.cumsum(to_blocks(decay_logarithm), axis=-1)
    causal = jnp.tril(jnp.ones((BLOCK, BLOCK), bool))
    strict = jnp.tril(jnp.ones((BLOCK, BLOCK), bool), -1)
    spread = cumulative[..., :, None] - cumulative[..., None, :]
    damping = jnp.where(causal, jnp.exp(jnp.where(causal, spread, 0.0)), 0.0)
    key_beta = key_block * beta_block[..., None]
    lower_part = jnp.einsum(
        "hnid,hnjd->hnij", key_beta, key_block, precision=PRECISION_FULL
    ) * jnp.where(strict, damping, 0.0)
    system = lower_part + jnp.eye(BLOCK, dtype=jnp.float32)
    right_side = jnp.concatenate(
        [value_block * beta_block[..., None], key_beta * jnp.exp(cumulative)[..., None]], axis=-1
    )
    solved = lax.linalg.triangular_solve(
        system, right_side, left_side=True, lower=True, unit_diagonal=True
    )
    target_values = solved[..., :head_width]
    householder_weights = solved[..., head_width:]
    inner_scores = (
        jnp.einsum("hnid,hnjd->hnij", query_block, key_block, precision=PRECISION_FULL) * damping
    )
    decayed_queries = query_block * jnp.exp(cumulative)[..., None]
    closing_log_decay = cumulative[..., -1:]
    decayed_keys = key_block * jnp.exp(closing_log_decay - cumulative)[..., None]
    return (
        decayed_queries,
        decayed_keys,
        target_values,
        householder_weights,
        inner_scores,
        closing_log_decay,
    )


def local_recurrence(
    query_projected,
    key_projected,
    value_projected,
    strength_logits,
    decay_preactivation,
    extra_log_decay,
    head_decay_rate,
):
    head_count = strength_logits.shape[0]
    tok_count = strength_logits.shape[1]

    def split_heads(tensor):
        return tensor.reshape(tok_count, head_count, HEAD).transpose(1, 0, 2).astype(jnp.float32)

    unit_queries = unit_rows(split_heads(query_projected)) * HEAD ** (-0.5)
    unit_keys = unit_rows(split_heads(key_projected))
    complete_values = split_heads(value_projected)
    score_terms = block_correction(
        unit_queries,
        unit_keys,
        complete_values,
        strength_logits,
        decay_preactivation,
        extra_log_decay,
        head_decay_rate,
    )
    identity = jnp.broadcast_to(jnp.eye(HEAD, dtype=jnp.float32), (head_count, HEAD, HEAD))

    def advance(carry, items):
        running_state, matrix_product = carry
        (
            decayed_queries,
            decayed_keys,
            target_values,
            householder_weights,
            inner_scores,
            closing_log_decay,
        ) = items
        new_state = target_values - jnp.einsum(
            "fdc,fcj->fdj", householder_weights, running_state, precision=PRECISION_FULL
        )
        layer_output = jnp.einsum(
            "fdc,fcj->fdj", decayed_queries, running_state, precision=PRECISION_FULL
        )
        layer_output = layer_output + jnp.einsum(
            "hij,hjv->hiv", inner_scores, new_state, precision=PRECISION_FULL
        )
        passed_state = decayed_queries - jnp.einsum(
            "hij,hjk->hik", inner_scores, householder_weights, precision=PRECISION_FULL
        )
        decay_span = jnp.einsum(
            "fdc,fcj->fdj", passed_state, matrix_product, precision=PRECISION_FULL
        )
        decay_factor = jnp.exp(closing_log_decay)[:, :, None]
        step_map = decay_factor * identity - jnp.einsum(
            "hik,hij->hkj", decayed_keys, householder_weights, precision=PRECISION_FULL
        )
        running_state = decay_factor * running_state + jnp.einsum(
            "xwp,xws->xps", decayed_keys, new_state, precision=PRECISION_FULL
        )
        matrix_product = jnp.einsum(
            "hij,hjk->hik", step_map, matrix_product, precision=PRECISION_FULL
        )
        return ((running_state, matrix_product), (layer_output, decay_span))

    moved = tuple((jnp.moveaxis(tensor, 1, 0) for tensor in score_terms))
    zeros_state = jnp.zeros((head_count, HEAD, HEAD), jnp.float32)
    (running_state, matrix_product), (block_outputs, decay_spans) = lax.scan(
        advance, (zeros_state, identity), moved
    )

    def merge_blocks(tensor):
        return jnp.moveaxis(tensor, 0, 1).reshape(head_count, tok_count, HEAD)

    return (
        merge_blocks(block_outputs),
        merge_blocks(decay_spans),
        matrix_product,
        running_state,
        identity,
    )


def feed_forward(whole_rows, gate_matrix, up_matrix, down_matrix):
    gate_whole, up_whole = (
        lax.all_gather(gate_matrix, "sp", axis=0, tiled=True),
        lax.all_gather(up_matrix, "sp", axis=0, tiled=True),
    )
    gate_total = jnp.dot(whole_rows, gate_whole, preferred_element_type=jnp.float32)
    up_total = jnp.dot(whole_rows, up_whole, preferred_element_type=jnp.float32)
    hidden = (jax.nn.silu(gate_total) * up_total).astype(jnp.bfloat16)
    down_whole = lax.all_gather(down_matrix, "sp", axis=1, tiled=True)
    return jnp.dot(hidden, down_whole, preferred_element_type=jnp.float32)


def body(
    stream,
    query_projected,
    key_projected,
    value_projected,
    gate_projected,
    strength_logits,
    decay_preactivation,
    extra_log_decay,
    head_decay_rate,
    head_norm_gain,
    head_output_matrix,
    feed_norm_gain,
    gate_matrix,
    up_matrix,
    down_matrix,
):
    block_outputs, decay_spans, matrix_product, running_state, identity = local_recurrence(
        query_projected,
        key_projected,
        value_projected,
        strength_logits,
        decay_preactivation,
        extra_log_decay,
        head_decay_rate,
    )
    zeros_state = jnp.zeros_like(running_state)

    def pass_state(turn, state_inflow):
        leaving = (
            jnp.einsum("hij,hjk->hik", matrix_product, state_inflow, precision=PRECISION_FULL)
            + running_state
        )
        return from_behind(leaving.astype(jnp.bfloat16), "sp", 1).astype(leaving.dtype)

    state_inflow = lax.fori_loop(0, lax.axis_size("sp") - 1, pass_state, zeros_state)
    attention_output = block_outputs + jnp.einsum(
        "qwc,qcn->qwn", decay_spans, state_inflow, precision=PRECISION_FULL
    )
    head_count = attention_output.shape[0]
    tok_count = attention_output.shape[1]
    normed_heads = rms_scale(attention_output) * head_norm_gain
    gated = normed_heads.transpose(1, 0, 2).reshape(tok_count, head_count * HEAD)
    mixed = (gated * jax.nn.silu(gate_projected.astype(jnp.float32))).astype(jnp.bfloat16)
    branch = lax.psum_scatter(
        jnp.dot(mixed, head_output_matrix, preferred_element_type=jnp.float32).astype(jnp.bfloat16),
        "tp",
        scatter_dimension=0,
        tiled=True,
    ).astype(jnp.float32)
    residual_own = stream.astype(jnp.float32) + branch
    normed_own = (rms_scale(residual_own) * feed_norm_gain).astype(jnp.bfloat16)
    whole_rows = lax.all_gather(normed_own, "tp", axis=0, tiled=True)
    ffn_term = feed_forward(whole_rows, gate_matrix, up_matrix, down_matrix)
    ffn_own = lax.psum_scatter(
        ffn_term.astype(jnp.bfloat16), "tp", scatter_dimension=0, tiled=True
    ).astype(jnp.float32)
    return (residual_own + ffn_own).astype(jnp.bfloat16)


def solution(mesh):
    placed = (
        P(("sp", "tp"), None),
        P("sp", "tp"),
        P("sp", "tp"),
        P("sp", "tp"),
        P("sp", "tp"),
        P("tp", "sp"),
        P("tp", "sp"),
        P("tp", "sp"),
        P("tp"),
        P(),
        P("tp", None),
        P(),
        P("sp", "tp"),
        P("sp", "tp"),
        P("tp", "sp"),
    )
    return jax.shard_map(
        body, mesh=mesh, in_specs=placed, out_specs=P(("sp", "tp"), None), check_vma=False
    )
```

profile of v0, /device:TPU:0, one launch (start us, length us, event | category | flops | bytes accessed | tf_op | source)
XLA Modules:
  0.0 551.2 jit_solution(7347479485389619198)
XLA Ops:
  8.9 1.1 fusion.64
  10.0 1.1 fusion.62
  11.1 1.1 fusion.60
  12.2 1.1 fusion.61
  16.0 59.6 %custom-call.3 = f32[2,6,1,64,64]{3,4,2,1,0:T(8,128)} custom-call(f32[2,6,1,64,64]{4,3,2,1,0:T(8,128)S(1)} %fusion.48), custom_call_target="InvertDiagBlocksLowerTriangular" | custom-call | tf_op jit(solution)/shard_map/triangular_solve | solution.py:63
  75.6 1.1 multiply_multiply_fusion
  79.3 36.4 %while.28 = (s32[]{:T(128)}, f32[2,128,128]{2,1,0:T(8,128)S(1)}, f32[2,128,128]{2,1,0:T(8,128)S(1)}, f32[6,2,64,128]{3,2,0,1:T(8,128)}, f32[6,2,64,128]{3,2,0,1:...) while((s32[]{:T(128)}, f32[2,128,128]{2,1,0:T(8,128)S(1)}, ...), condition=%wide.region_4.5_spmd.clone, body=%wide.region_3.4_spmd.clone.sunk | while | flops 201605120 | bytes 2759337 | solution.py:152
  79.4 1.1 convolution_subtract_fusion.6
  80.5 1.1 fusion.145
  85.4 1.1 convolution_subtract_fusion.6
  86.5 1.1 fusion.145
  91.5 1.1 convolution_subtract_fusion.6
  92.6 1.1 fusion.145
  97.5 1.1 convolution_subtract_fusion.6
  98.6 1.1 fusion.145
  103.6 1.1 convolution_subtract_fusion.6
  104.7 1.1 fusion.145
  109.7 1.1 convolution_subtract_fusion.6
  110.7 1.1 fusion.145
  113.1 1.0 convolution_subtract_fusion.8
  115.7 1.2 copy.42
  116.9 49.8 %while.29 = (s32[]{:T(128)}, f32[2,128,128]{2,1,0:T(8,128)S(1)}, f32[2,128,128]{2,1,0:T(8,128)S(1)}, f32[2,128,128]{2,1,0:T(8,128)S(1)}, s32[]{:T(128)}, /*index=5*/s32[]{:T(128)}) while((s32[]{:T(128)}, f32[2,128,128]{2,1,0:T(8,128)S(1)}, f32[2,128,128]{2,1,0:T(8,128)S(1)}, f32[2,128,128]{2,1,0:T(8,128)S(1)}, s32[]{:T(128)}, ...), condition=%wide.region_6.7_spmd.clone, body=%wide.region_5.6_spmd.clone.sunk | while | flops 50462720 | bytes 917623 | solution.py:215
  117.2 4.9 collective-permute-start
  122.1 1.9 collective-permute-done
  124.3 4.3 collective-permute-start
  128.6 1.9 collective-permute-done
  130.8 4.3 collective-permute-start
  135.1 1.9 collective-permute-done
  137.3 5.2 collective-permute-start
  142.5 1.9 collective-permute-done
  144.7 5.2 collective-permute-start
  149.9 1.9 collective-permute-done
  152.1 5.3 collective-permute-start
  157.3 2.1 collective-permute-done
  159.7 5.1 collective-permute-start
  164.8 1.9 collective-permute-done
  167.8 1.8 convolution_convert_fusion.1
  169.6 31.9 %reduce-scatter.3.cloned.1.call-done = bf16[96,2048]{1,0:T(8,128)(2,1)} async-done(((bf16[384,2048]{1,0:T(8,128)(2,1)}), bf16[96,2048]{1,0:T(8,128)(2,1)}) %reduce-scatter.3.cloned.1.call-update) | async-done | bytes 393232 | tf_op jit(solution)/shard_map/reduce_scatter | solution.py:224
  201.5 1.2 multiply_reduce_fusion
  202.8 1.9 multiply_convert_fusion
  206.8 17.7 %all-gather.5.cloned.1.call-done = bf16[384,2048]{1,0:T(8,128)(2,1)} async-done(((bf16[96,2048]{1,0:T(8,128)(2,1)}), bf16[384,2048]{1,0:T(8,128)(2,1)}) %all-gather.5.cloned.1.call-update) | async-done | bytes 1572880 | tf_op jit(solution)/shard_map/all_gather | solution.py:232
  224.5 94.5 %all-gather.7.cloned.1.call-done = bf16[2048,1408]{1,0:T(8,128)(2,1)} async-done(((bf16[256,1408]{1,0:T(8,128)(2,1)}), bf16[2048,1408]{1,0:T(8,128)(2,1)}) %all-gather.7.cloned.1.call-update) | async-done | bytes 5767184 | tf_op jit(solution)/shard_map/all_gather | solution.py:170
  319.0 7.1 %fusion.84 = f32[384,1408]{1,0:T(8,128)} fusion(bf16[384,2048]{1,0:T(8,128)(2,1)} %all-gather.5.cloned.1.call-done, bf16[2048,1408]{1,0:T(8,128)(2,1)} %all-gather.7.cloned.1.call-done), kind=kOutput, calls=%fused_computation.133 | convolution fusion | flops 2214592512 | bytes 9502720 | tf_op jit(solution)/shard_map/dot_general | solution.py:173
  326.1 86.2 %all-gather.11.cloned.1.call-done = bf16[1408,2048]{1,0:T(8,128)(2,1)} async-done(((bf16[1408,256]{1,0:T(8,128)(2,1)}), bf16[1408,2048]{1,0:T(8,128)(2,1)}) %all-gather.11.cloned.1.call-update) | async-done | bytes 5767184 | tf_op jit(solution)/shard_map/all_gather | solution.py:176
  412.3 92.6 %all-gather.9.cloned.1.call-done = bf16[2048,1408]{1,0:T(8,128)(2,1)} async-done(((bf16[256,1408]{1,0:T(8,128)(2,1)}), bf16[2048,1408]{1,0:T(8,128)(2,1)}) %all-gather.9.cloned.1.call-update) | async-done | bytes 5767184 | tf_op jit(solution)/shard_map/all_gather | solution.py:171
  504.8 11.3 %convolution_convert_fusion = bf16[384,2048]{1,0:T(8,128)(2,1)} fusion(bf16[1408,2048]{1,0:T(8,128)(2,1)} %all-gather.11.cloned.1.call-done, bf16[384,2048]{1,0:T(8,128)(2,1)S(1)} %copy-done.7, bf16[2048,1408]{1,0:T(8,128)(2,1)} %all-gather.9.cloned.1.call-done, f32[384,1408]{1,0:T(8,128)} %fusion.84), kind=kOutput, calls=%fused_computation.52 | convolution fusion | flops 4433215488 | bytes 16842752 | tf_op jit(solution)/shard_map/dot_general | solution.py:177
  516.1 26.4 %reduce-scatter.5.cloned.1.call-done = bf16[96,2048]{1,0:T(8,128)(2,1)} async-done(((bf16[384,2048]{1,0:T(8,128)(2,1)}), bf16[96,2048]{1,0:T(8,128)(2,1)}) %reduce-scatter.5.cloned.1.call-update) | async-done | bytes 393232 | tf_op jit(solution)/shard_map/reduce_scatter | solution.py:234
  542.5 1.9 add_convert_fusion
  (121 shorter events, 34.4 us)
Async XLA Ops:
  6.5 161.2 %copy-start = (bf16[256,2048]{1,0:T(8,128)(2,1)S(1)}, bf16[256,2048]{1,0:T(8,128)(2,1)}, u32[]{:S(2)}) copy-start(bf16[256,2048]{1,0:T(8,128)(2,1)} %param.29) | copy-start | bytes 3145732
  6.5 195.0 %reduce-scatter.3.cloned.1.call-start = ((), (), s32[]{:S(2)}) async-start(), calls=%async_computation.2 | async-start | bytes 1966080 | tf_op jit(solution)/shard_map/reduce_scatter | solution.py:224
  75.6 1.1 copy-start.4
  115.7 51.0 %copy-start.3 = (f32[6,2,64,128]{3,2,0,1:T(8,128)S(1)}, f32[6,2,64,128]{3,2,0,1:T(8,128)}, u32[]{:S(2)}) copy-start(f32[6,2,64,128]{3,2,0,1:T(8,128)} %get-tuple-element.93) | copy-start | bytes 1179652
  116.9 50.5 %copy-start.6 = (f32[128]{0:T(128)S(1)}, f32[128]{0:T(128)}, u32[]{:S(2)}) copy-start(f32[128]{0:T(128)} %param.28) | copy-start | bytes 1540
  117.2 6.8 %collective-permute-start = (bf16[2,128,128]{2,1,0:T(8,128)(2,1)S(1)}, bf16[2,128,128]{2,1,0:T(8,128)(2,1)S(1)}, u32[]{:S(2)}, u32[]{:S(2)}) collective-permute-start(bf16[2,128,128]{2,1,0:T(8,128)(2,1)S(1)} %fusion.150), channel_id=1, source_target_pairs={{0,4},{4,8},{8,12},{12,16},{16,20},{20,24},{24,28},{1,5},{5,9},{9,... | collective-permute-start | bytes 196616 | tf_op jit(solution)/shard_map/while/body/eval_jaxpr/ppermute | solution.py:15
  124.3 6.2 %collective-permute-start = (bf16[2,128,128]{2,1,0:T(8,128)(2,1)S(1)}, bf16[2,128,128]{2,1,0:T(8,128)(2,1)S(1)}, u32[]{:S(2)}, u32[]{:S(2)}) collective-permute-start(bf16[2,128,128]{2,1,0:T(8,128)(2,1)S(1)} %fusion.150), channel_id=1, source_target_pairs={{0,4},{4,8},{8,12},{12,16},{16,20},{20,24},{24,28},{1,5},{5,9},{9,... | collective-permute-start | bytes 196616 | tf_op jit(solution)/shard_map/while/body/eval_jaxpr/ppermute | solution.py:15
  130.8 6.2 %collective-permute-start = (bf16[2,128,128]{2,1,0:T(8,128)(2,1)S(1)}, bf16[2,128,128]{2,1,0:T(8,128)(2,1)S(1)}, u32[]{:S(2)}, u32[]{:S(2)}) collective-permute-start(bf16[2,128,128]{2,1,0:T(8,128)(2,1)S(1)} %fusion.150), channel_id=1, source_target_pairs={{0,4},{4,8},{8,12},{12,16},{16,20},{20,24},{24,28},{1,5},{5,9},{9,... | collective-permute-start | bytes 196616 | tf_op jit(solution)/shard_map/while/body/eval_jaxpr/ppermute | solution.py:15
  137.3 7.1 %collective-permute-start = (bf16[2,128,128]{2,1,0:T(8,128)(2,1)S(1)}, bf16[2,128,128]{2,1,0:T(8,128)(2,1)S(1)}, u32[]{:S(2)}, u32[]{:S(2)}) collective-permute-start(bf16[2,128,128]{2,1,0:T(8,128)(2,1)S(1)} %fusion.150), channel_id=1, source_target_pairs={{0,4},{4,8},{8,12},{12,16},{16,20},{20,24},{24,28},{1,5},{5,9},{9,... | collective-permute-start | bytes 196616 | tf_op jit(solution)/shard_map/while/body/eval_jaxpr/ppermute | solution.py:15
  144.7 7.1 %collective-permute-start = (bf16[2,128,128]{2,1,0:T(8,128)(2,1)S(1)}, bf16[2,128,128]{2,1,0:T(8,128)(2,1)S(1)}, u32[]{:S(2)}, u32[]{:S(2)}) collective-permute-start(bf16[2,128,128]{2,1,0:T(8,128)(2,1)S(1)} %fusion.150), channel_id=1, source_target_pairs={{0,4},{4,8},{8,12},{12,16},{16,20},{20,24},{24,28},{1,5},{5,9},{9,... | collective-permute-start | bytes 196616 | tf_op jit(solution)/shard_map/while/body/eval_jaxpr/ppermute | solution.py:15
  152.1 7.4 %collective-permute-start = (bf16[2,128,128]{2,1,0:T(8,128)(2,1)S(1)}, bf16[2,128,128]{2,1,0:T(8,128)(2,1)S(1)}, u32[]{:S(2)}, u32[]{:S(2)}) collective-permute-start(bf16[2,128,128]{2,1,0:T(8,128)(2,1)S(1)} %fusion.150), channel_id=1, source_target_pairs={{0,4},{4,8},{8,12},{12,16},{16,20},{20,24},{24,28},{1,5},{5,9},{9,... | collective-permute-start | bytes 196616 | tf_op jit(solution)/shard_map/while/body/eval_jaxpr/ppermute | solution.py:15
  159.7 7.0 %collective-permute-start = (bf16[2,128,128]{2,1,0:T(8,128)(2,1)S(1)}, bf16[2,128,128]{2,1,0:T(8,128)(2,1)S(1)}, u32[]{:S(2)}, u32[]{:S(2)}) collective-permute-start(bf16[2,128,128]{2,1,0:T(8,128)(2,1)S(1)} %fusion.150), channel_id=1, source_target_pairs={{0,4},{4,8},{8,12},{12,16},{16,20},{20,24},{24,28},{1,5},{5,9},{9,... | collective-permute-start | bytes 196616 | tf_op jit(solution)/shard_map/while/body/eval_jaxpr/ppermute | solution.py:15
  166.7 1.0 copy-start.8
  167.7 33.8 %copy-start.1 = (bf16[96,2048]{1,0:T(8,128)(2,1)S(1)}, bf16[96,2048]{1,0:T(8,128)(2,1)}, u32[]{:S(2)}) copy-start(bf16[96,2048]{1,0:T(8,128)(2,1)} %param.19) | copy-start | bytes 1179652
  167.7 35.0 %copy-start.5 = (f32[2048]{0:T(1024)S(1)}, f32[2048]{0:T(1024)}, u32[]{:S(2)}) copy-start(f32[2048]{0:T(1024)} %param.30) | copy-start | bytes 24580
  169.6 54.9 %all-gather.5.cloned.1.call-start = ((), (), s32[]{:S(2)}) async-start(), calls=%async_computation.3 | async-start | bytes 1966080 | tf_op jit(solution)/shard_map/all_gather | solution.py:232
  204.7 114.3 %all-gather.7.cloned.1.call-start = ((), (), s32[]{:S(2)}) async-start(), calls=%async_computation.4 | async-start | bytes 6488064 | tf_op jit(solution)/shard_map/all_gather | solution.py:170
  205.4 206.8 %all-gather.11.cloned.1.call-start = ((), (), s32[]{:S(2)}) async-start(), calls=%async_computation.6 | async-start | bytes 6488064 | tf_op jit(solution)/shard_map/all_gather | solution.py:176
  206.0 298.8 %all-gather.9.cloned.1.call-start = ((), (), s32[]{:S(2)}) async-start(), calls=%async_computation.5 | async-start | bytes 6488064 | tf_op jit(solution)/shard_map/all_gather | solution.py:171
  206.6 335.9 %reduce-scatter.5.cloned.1.call-start = ((), (), s32[]{:S(2)}) async-start(), calls=%async_computation.7 | async-start | bytes 1966080 | tf_op jit(solution)/shard_map/reduce_scatter | solution.py:234
  224.5 280.3 %copy-start.7 = (bf16[384,2048]{1,0:T(8,128)(2,1)S(1)}, bf16[384,2048]{1,0:T(8,128)(2,1)}, u32[]{:S(2)}) copy-start(bf16[384,2048]{1,0:T(8,128)(2,1)} %all-gather.5.cloned.1.call-done) | copy-start | bytes 4718596
  326.1 216.4 %copy-start.2 = (bf16[96,2048]{1,0:T(8,128)(2,1)S(1)}, bf16[96,2048]{1,0:T(8,128)(2,1)}, u32[]{:S(2)}) copy-start(bf16[96,2048]{1,0:T(8,128)(2,1)} %reduce-scatter.3.cloned.1.call-done) | copy-start | bytes 1179652
Sparse Core Ops, SparseCore 0:
  169.7 31.7 reduce-scatter.2
  204.8 19.6 all-gather.4
  226.7 92.3 all-gather.6
  320.9 91.2 all-gather.10
  414.3 90.4 all-gather.8
  516.2 26.1 reduce-scatter.4
where the time goes:
time: 553 us; the launch traced here: 551 us
  waiting for transfers between devices  364 us (66%)
  other arithmetic  74.1 us (13%)
  matrix products  60.9 us (11%)
  starting transfers between devices  34.5 us (6%)
  between operations  13.7 us (2%)
    all_gather x1, waiting for transfers between devices, feed_forward(): lax.all_gather(gate_matrix, 'sp', axis=0, tiled=True)  94.5 us
    all_gather x1, waiting for transfers between devices, feed_forward(): lax.all_gather(up_matrix, 'sp', axis=0, tiled=True)  92.6 us
    all_gather x1, waiting for transfers between devices, feed_forward(): down_whole = lax.all_gather(down_matrix, 'sp', axis=1, tiled=True)  86.2 us
    another operation x2, other arithmetic, block_correction(): lax.linalg.triangular_solve(system, right_side, left_side=True, lower=Tru...  59.6 us
    ppermute x7, starting transfers between devices, from_behind(): return lax.ppermute(value, axis, pairs)  34.2 us
    reduce_scatter x1, waiting for transfers between devices, body(): lax.psum_scatter(jnp.dot(mixed, head_output_matrix, preferred_element_typ...  31.9 us
    reduce_scatter x1, waiting for transfers between devices, body(): lax.psum_scatter(ffn_term.astype(jnp.bfloat16), 'tp', scatter_dimension=0...  26.4 us
    all_gather x1, waiting for transfers between devices, body(): whole_rows = lax.all_gather(normed_own, 'tp', axis=0, tiled=True)  17.7 us
  transfers between devices with their start and end apart: 13, of which 13 were waited for; matrix products, arithmetic and copies ran while one was open for 1% of the time, Pallas kernels for 0%

commit v1 on v0

--- a/solution.py
+++ b/solution.py
@@ -173,7 +173,7 @@
     gate_total = jnp.dot(whole_rows, gate_whole, preferred_element_type=jnp.float32)
     up_total = jnp.dot(whole_rows, up_whole, preferred_element_type=jnp.float32)
     hidden = (jax.nn.silu(gate_total) * up_total).astype(jnp.bfloat16)
-    down_whole = lax.all_gather(down_matrix, "sp", axis=1, tiled=True)
+    down_whole = jnp.concatenate(lax.all_gather(down_matrix, "sp"), axis=1)
     return jnp.dot(hidden, down_whole, preferred_element_type=jnp.float32)
 
 

time: 553 us -> 524 us (0.948)
  waiting for transfers between devices: 364 us -> 325 us
  local copies, waits for them, and re-layouts: 2.78 us -> 11.1 us
    all_gather x1, waiting for transfers between devices: 86.2 us -> 61.9 us  [feed_forward(): down_whole = jnp.concatenate(lax.all_gather(down_matrix, 'sp'), axis=1)]
    reshape x0 -> x1, local copies, waits for them, and re-layouts: none -> 8.34 us  [feed_forward(): down_whole = jnp.concatenate(lax.all_gather(down_matrix, 'sp'), axis=1)]
    all_gather x1, waiting for transfers between devices: 92.6 us -> 85.3 us  [feed_forward(): lax.all_gather(up_matrix, 'sp', axis=0, tiled=True)]
    all_gather x1, waiting for transfers between devices: 17.7 us -> 10.7 us  [body(): whole_rows = lax.all_gather(normed_own, 'tp', axis=0, tiled=True)]
  transfers between devices with their start and end apart: 13 -> 13, of which waited for: 13 -> 13; matrix products, arithmetic and copies ran while one was open for 1% -> 4% of each run, Pallas kernels for 0% -> 0%
where the time goes in v1:
time: 524 us; the launch traced here: 522 us
  waiting for transfers between devices  325 us (62%)
  other arithmetic  74.2 us (14%)
  matrix products  61 us (12%)
  starting transfers between devices  34.5 us (7%)
  between operations  15.3 us (3%)
  local copies, waits for them, and re-layouts  11.1 us (2%)
    all_gather x1, waiting for transfers between devices, feed_forward(): lax.all_gather(gate_matrix, 'sp', axis=0, tiled=True)  94.2 us
    all_gather x1, waiting for transfers between devices, feed_forward(): lax.all_gather(up_matrix, 'sp', axis=0, tiled=True)  85.3 us
    all_gather x1, waiting for transfers between devices, feed_forward(): down_whole = jnp.concatenate(lax.all_gather(down_matrix, 'sp'), axis=1)  61.9 us
    another operation x2, other arithmetic, block_correction(): lax.linalg.triangular_solve(system, right_side, left_side=True, lower=Tru...  59.6 us
    ppermute x7, starting transfers between devices, from_behind(): return lax.ppermute(value, axis, pairs)  34.2 us
    reduce_scatter x1, waiting for transfers between devices, body(): lax.psum_scatter(jnp.dot(mixed, head_output_matrix, preferred_element_typ...  31.3 us
    reduce_scatter x1, waiting for transfers between devices, body(): lax.psum_scatter(ffn_term.astype(jnp.bfloat16), 'tp', scatter_dimension=0...  26.4 us
    ppermute x7, waiting for transfers between devices, from_behind(): return lax.ppermute(value, axis, pairs)  13.4 us
  transfers between devices with their start and end apart: 13, of which 13 were waited for; matrix products, arithmetic and copies ran while one was open for 4% of the time, Pallas kernels for 0%

profile of v1, /device:TPU:0, one launch (start us, length us, event | category | flops | bytes accessed | tf_op | source)
XLA Modules:
  0.0 521.9 jit_solution(3108760313086860133)
XLA Ops:
  9.7 1.1 fusion.64
  10.8 1.1 fusion.62
  11.9 1.1 fusion.60
  13.1 1.1 fusion.61
  16.8 59.6 %custom-call.3 = f32[2,6,1,64,64]{3,4,2,1,0:T(8,128)} custom-call(f32[2,6,1,64,64]{4,3,2,1,0:T(8,128)S(1)} %fusion.48), custom_call_target="InvertDiagBlocksLowerTriangular" | custom-call | tf_op jit(solution)/shard_map/triangular_solve | solution.py:63
  76.4 1.1 multiply_multiply_fusion
  80.2 36.4 %while.28 = (s32[]{:T(128)}, f32[2,128,128]{2,1,0:T(8,128)S(1)}, f32[2,128,128]{2,1,0:T(8,128)S(1)}, f32[6,2,64,128]{3,2,0,1:T(8,128)}, f32[6,2,64,128]{3,2,0,1:...) while((s32[]{:T(128)}, f32[2,128,128]{2,1,0:T(8,128)S(1)}, ...), condition=%wide.region_4.5_spmd.clone, body=%wide.region_3.4_spmd.clone.sunk | while | flops 201605120 | bytes 2759337 | solution.py:152
  80.2 1.1 convolution_subtract_fusion.6
  81.3 1.1 fusion.145
  86.3 1.1 convolution_subtract_fusion.6
  87.3 1.1 fusion.145
  92.3 1.1 convolution_subtract_fusion.6
  93.4 1.1 fusion.145
  98.4 1.1 convolution_subtract_fusion.6
  99.5 1.1 fusion.145
  104.4 1.1 convolution_subtract_fusion.6
  105.5 1.1 fusion.145
  110.5 1.1 convolution_subtract_fusion.6
  111.6 1.1 fusion.145
  116.5 1.2 copy.57
  117.8 49.8 %while.29 = (s32[]{:T(128)}, f32[2,128,128]{2,1,0:T(8,128)S(1)}, f32[2,128,128]{2,1,0:T(8,128)S(1)}, f32[2,128,128]{2,1,0:T(8,128)S(1)}, s32[]{:T(128)}, /*index=5*/s32[]{:T(128)}) while((s32[]{:T(128)}, f32[2,128,128]{2,1,0:T(8,128)S(1)}, f32[2,128,128]{2,1,0:T(8,128)S(1)}, f32[2,128,128]{2,1,0:T(8,128)S(1)}, s32[]{:T(128)}, ...), condition=%wide.region_6.7_spmd.clone, body=%wide.region_5.6_spmd.clone.sunk | while | flops 50462720 | bytes 917623 | solution.py:215
  118.1 4.9 collective-permute-start
  123.0 1.9 collective-permute-done
  125.2 4.3 collective-permute-start
  129.4 1.9 collective-permute-done
  131.6 4.3 collective-permute-start
  136.0 1.9 collective-permute-done
  138.2 5.2 collective-permute-start
  143.3 1.9 collective-permute-done
  145.5 5.2 collective-permute-start
  150.7 1.9 collective-permute-done
  152.9 5.3 %collective-permute-start = (bf16[2,128,128]{2,1,0:T(8,128)(2,1)S(1)}, bf16[2,128,128]{2,1,0:T(8,128)(2,1)S(1)}, u32[]{:S(2)}, u32[]{:S(2)}) collective-permute-start(bf16[2,128,128]{2,1,0:T(8,128)(2,1)S(1)} %fusion.150), channel_id=1, source_target_pairs={{0,4},{4,8},{8,12},{12,16},{16,20},{20,24},{24,28},{1,5},{5,9},{9,... | collective-permute-start | bytes 196616 | tf_op jit(solution)/shard_map/while/body/eval_jaxpr/ppermute | solution.py:15
  158.2 2.1 collective-permute-done
  160.6 5.1 collective-permute-start
  165.7 1.9 collective-permute-done
  168.6 1.8 convolution_convert_fusion.1
  171.0 31.3 %reduce-scatter.3.cloned.1.call-done = bf16[96,2048]{1,0:T(8,128)(2,1)} async-done(((bf16[384,2048]{1,0:T(8,128)(2,1)}), bf16[96,2048]{1,0:T(8,128)(2,1)}) %reduce-scatter.3.cloned.1.call-update) | async-done | bytes 393232 | tf_op jit(solution)/shard_map/reduce_scatter | solution.py:224
  202.4 1.2 multiply_reduce_fusion
  203.6 1.9 multiply_convert_fusion
  207.1 61.9 %all-gather.12.cloned.1.call-done = bf16[11264,256]{1,0:T(8,128)(2,1)} async-done(((bf16[1408,256]{1,0:T(8,128)(2,1)}), bf16[11264,256]{1,0:T(8,128)(2,1)}) %all-gather.12.cloned.1.call-update) | async-done | bytes 5767184 | tf_op jit(solution)/shard_map/all_gather | solution.py:176
  269.0 8.3 %copy.59 = bf16[1408,8,256]{0,2,1:T(8,128)(2,1)} copy(bf16[1408,8,256]{2,0,1:T(8,128)(2,1)} %bitcast.192) | data formatting | bytes 11534336 | tf_op jit(solution)/shard_map/reshape | solution.py:176
  277.4 10.7 %all-gather.6.cloned.1.call-done = bf16[384,2048]{1,0:T(8,128)(2,1)} async-done(((bf16[96,2048]{1,0:T(8,128)(2,1)}), bf16[384,2048]{1,0:T(8,128)(2,1)}) %all-gather.6.cloned.1.call-update) | async-done | bytes 1572880 | tf_op jit(solution)/shard_map/all_gather | solution.py:232
  288.1 94.2 %all-gather.8.cloned.1.call-done = bf16[2048,1408]{1,0:T(8,128)(2,1)} async-done(((bf16[256,1408]{1,0:T(8,128)(2,1)}), bf16[2048,1408]{1,0:T(8,128)(2,1)}) %all-gather.8.cloned.1.call-update) | async-done | bytes 5767184 | tf_op jit(solution)/shard_map/all_gather | solution.py:170
  382.3 7.2 %fusion.84 = f32[384,1408]{1,0:T(8,128)} fusion(bf16[384,2048]{1,0:T(8,128)(2,1)} %all-gather.6.cloned.1.call-done, bf16[2048,1408]{1,0:T(8,128)(2,1)} %all-gather.8.cloned.1.call-done), kind=kOutput, calls=%fused_computation.133 | convolution fusion | flops 2214592512 | bytes 9502720 | tf_op jit(solution)/shard_map/dot_general | solution.py:173
  389.5 85.3 %all-gather.10.cloned.1.call-done = bf16[2048,1408]{1,0:T(8,128)(2,1)} async-done(((bf16[256,1408]{1,0:T(8,128)(2,1)}), bf16[2048,1408]{1,0:T(8,128)(2,1)}) %all-gather.10.cloned.1.call-update) | async-done | bytes 5767184 | tf_op jit(solution)/shard_map/all_gather | solution.py:171
  474.9 11.2 %convolution_convert_fusion = bf16[384,2048]{1,0:T(8,128)(2,1)} fusion(bf16[1408,2048]{0,1:T(8,128)(2,1)} %bitcast.193, bf16[384,2048]{1,0:T(8,128)(2,1)S(1)} %copy-done.7, bf16[2048,1408]{1,0:T(8,128)(2,1)} %all-gather.10.cloned.1.call-done, f32[384,1408]{1,0:T(8,128)} %fusion.84), kind=kOutput, calls=%fused_computation.52 | convolution fusion | flops 4433215488 | bytes 16842752 | tf_op jit(solution)/shard_map/dot_general | solution.py:177
  486.1 26.4 %reduce-scatter.5.cloned.1.call-done = bf16[96,2048]{1,0:T(8,128)(2,1)} async-done(((bf16[384,2048]{1,0:T(8,128)(2,1)}), bf16[96,2048]{1,0:T(8,128)(2,1)}) %reduce-scatter.5.cloned.1.call-update) | async-done | bytes 393232 | tf_op jit(solution)/shard_map/reduce_scatter | solution.py:234
  512.4 1.9 add_convert_fusion
  (122 shorter events, 35.5 us)
Async XLA Ops:
  7.4 161.2 %copy-start = (bf16[256,2048]{1,0:T(8,128)(2,1)S(1)}, bf16[256,2048]{1,0:T(8,128)(2,1)}, u32[]{:S(2)}) copy-start(bf16[256,2048]{1,0:T(8,128)(2,1)} %param.29) | copy-start | bytes 3145732
  7.4 195.0 %reduce-scatter.3.cloned.1.call-start = ((), (), s32[]{:S(2)}) async-start(), calls=%async_computation.2 | async-start | bytes 1966080 | tf_op jit(solution)/shard_map/reduce_scatter | solution.py:224
  76.4 1.1 copy-start.4
  116.5 51.0 %copy-start.3 = (f32[6,2,64,128]{3,2,0,1:T(8,128)S(1)}, f32[6,2,64,128]{3,2,0,1:T(8,128)}, u32[]{:S(2)}) copy-start(f32[6,2,64,128]{3,2,0,1:T(8,128)} %get-tuple-element.93) | copy-start | bytes 1179652
  117.8 50.5 %copy-start.6 = (f32[128]{0:T(128)S(1)}, f32[128]{0:T(128)}, u32[]{:S(2)}) copy-start(f32[128]{0:T(128)} %param.28) | copy-start | bytes 1540
  118.1 6.8 %collective-permute-start = (bf16[2,128,128]{2,1,0:T(8,128)(2,1)S(1)}, bf16[2,128,128]{2,1,0:T(8,128)(2,1)S(1)}, u32[]{:S(2)}, u32[]{:S(2)}) collective-permute-start(bf16[2,128,128]{2,1,0:T(8,128)(2,1)S(1)} %fusion.150), channel_id=1, source_target_pairs={{0,4},{4,8},{8,12},{12,16},{16,20},{20,24},{24,28},{1,5},{5,9},{9,... | collective-permute-start | bytes 196616 | tf_op jit(solution)/shard_map/while/body/eval_jaxpr/ppermute | solution.py:15
  125.2 6.2 %collective-permute-start = (bf16[2,128,128]{2,1,0:T(8,128)(2,1)S(1)}, bf16[2,128,128]{2,1,0:T(8,128)(2,1)S(1)}, u32[]{:S(2)}, u32[]{:S(2)}) collective-permute-start(bf16[2,128,128]{2,1,0:T(8,128)(2,1)S(1)} %fusion.150), channel_id=1, source_target_pairs={{0,4},{4,8},{8,12},{12,16},{16,20},{20,24},{24,28},{1,5},{5,9},{9,... | collective-permute-start | bytes 196616 | tf_op jit(solution)/shard_map/while/body/eval_jaxpr/ppermute | solution.py:15
  131.6 6.2 %collective-permute-start = (bf16[2,128,128]{2,1,0:T(8,128)(2,1)S(1)}, bf16[2,128,128]{2,1,0:T(8,128)(2,1)S(1)}, u32[]{:S(2)}, u32[]{:S(2)}) collective-permute-start(bf16[2,128,128]{2,1,0:T(8,128)(2,1)S(1)} %fusion.150), channel_id=1, source_target_pairs={{0,4},{4,8},{8,12},{12,16},{16,20},{20,24},{24,28},{1,5},{5,9},{9,... | collective-permute-start | bytes 196616 | tf_op jit(solution)/shard_map/while/body/eval_jaxpr/ppermute | solution.py:15
  138.2 7.1 %collective-permute-start = (bf16[2,128,128]{2,1,0:T(8,128)(2,1)S(1)}, bf16[2,128,128]{2,1,0:T(8,128)(2,1)S(1)}, u32[]{:S(2)}, u32[]{:S(2)}) collective-permute-start(bf16[2,128,128]{2,1,0:T(8,128)(2,1)S(1)} %fusion.150), channel_id=1, source_target_pairs={{0,4},{4,8},{8,12},{12,16},{16,20},{20,24},{24,28},{1,5},{5,9},{9,... | collective-permute-start | bytes 196616 | tf_op jit(solution)/shard_map/while/body/eval_jaxpr/ppermute | solution.py:15
  145.5 7.1 %collective-permute-start = (bf16[2,128,128]{2,1,0:T(8,128)(2,1)S(1)}, bf16[2,128,128]{2,1,0:T(8,128)(2,1)S(1)}, u32[]{:S(2)}, u32[]{:S(2)}) collective-permute-start(bf16[2,128,128]{2,1,0:T(8,128)(2,1)S(1)} %fusion.150), channel_id=1, source_target_pairs={{0,4},{4,8},{8,12},{12,16},{16,20},{20,24},{24,28},{1,5},{5,9},{9,... | collective-permute-start | bytes 196616 | tf_op jit(solution)/shard_map/while/body/eval_jaxpr/ppermute | solution.py:15
  152.9 7.4 %collective-permute-start = (bf16[2,128,128]{2,1,0:T(8,128)(2,1)S(1)}, bf16[2,128,128]{2,1,0:T(8,128)(2,1)S(1)}, u32[]{:S(2)}, u32[]{:S(2)}) collective-permute-start(bf16[2,128,128]{2,1,0:T(8,128)(2,1)S(1)} %fusion.150), channel_id=1, source_target_pairs={{0,4},{4,8},{8,12},{12,16},{16,20},{20,24},{24,28},{1,5},{5,9},{9,... | collective-permute-start | bytes 196616 | tf_op jit(solution)/shard_map/while/body/eval_jaxpr/ppermute | solution.py:15
  160.6 7.0 %collective-permute-start = (bf16[2,128,128]{2,1,0:T(8,128)(2,1)S(1)}, bf16[2,128,128]{2,1,0:T(8,128)(2,1)S(1)}, u32[]{:S(2)}, u32[]{:S(2)}) collective-permute-start(bf16[2,128,128]{2,1,0:T(8,128)(2,1)S(1)} %fusion.150), channel_id=1, source_target_pairs={{0,4},{4,8},{8,12},{12,16},{16,20},{20,24},{24,28},{1,5},{5,9},{9,... | collective-permute-start | bytes 196616 | tf_op jit(solution)/shard_map/while/body/eval_jaxpr/ppermute | solution.py:15
  167.6 1.0 copy-start.8
  168.6 33.8 %copy-start.1 = (bf16[96,2048]{1,0:T(8,128)(2,1)S(1)}, bf16[96,2048]{1,0:T(8,128)(2,1)}, u32[]{:S(2)}) copy-start(bf16[96,2048]{1,0:T(8,128)(2,1)} %param.19) | copy-start | bytes 1179652
  170.4 33.2 %copy-start.5 = (f32[2048]{0:T(1024)S(1)}, f32[2048]{0:T(1024)}, u32[]{:S(2)}) copy-start(f32[2048]{0:T(1024)} %param.30) | copy-start | bytes 24580
  170.4 98.6 %all-gather.12.cloned.1.call-start = ((), (), s32[]{:S(2)}) async-start(), calls=%async_computation.7 | async-start | bytes 6488064 | tf_op jit(solution)/shard_map/all_gather | solution.py:176
  171.0 117.1 %all-gather.6.cloned.1.call-start = ((), (), s32[]{:S(2)}) async-start(), calls=%async_computation.3 | async-start | bytes 1966080 | tf_op jit(solution)/shard_map/all_gather | solution.py:232
  205.5 176.8 %all-gather.8.cloned.1.call-start = ((), (), s32[]{:S(2)}) async-start(), calls=%async_computation.4 | async-start | bytes 6488064 | tf_op jit(solution)/shard_map/all_gather | solution.py:170
  206.1 268.7 %all-gather.10.cloned.1.call-start = ((), (), s32[]{:S(2)}) async-start(), calls=%async_computation.5 | async-start | bytes 6488064 | tf_op jit(solution)/shard_map/all_gather | solution.py:171
  206.9 305.6 %reduce-scatter.5.cloned.1.call-start = ((), (), s32[]{:S(2)}) async-start(), calls=%async_computation.6 | async-start | bytes 1966080 | tf_op jit(solution)/shard_map/reduce_scatter | solution.py:234
  288.1 186.7 %copy-start.7 = (bf16[384,2048]{1,0:T(8,128)(2,1)S(1)}, bf16[384,2048]{1,0:T(8,128)(2,1)}, u32[]{:S(2)}) copy-start(bf16[384,2048]{1,0:T(8,128)(2,1)} %all-gather.6.cloned.1.call-done) | copy-start | bytes 4718596
  474.9 37.6 %copy-start.2 = (bf16[96,2048]{1,0:T(8,128)(2,1)S(1)}, bf16[96,2048]{1,0:T(8,128)(2,1)}, u32[]{:S(2)}) copy-start(bf16[96,2048]{1,0:T(8,128)(2,1)} %reduce-scatter.3.cloned.1.call-done) | copy-start | bytes 1179652
Sparse Core Ops, SparseCore 0:
  170.5 31.7 reduce-scatter.2
  486.2 26.1 reduce-scatter.4
Sparse Core Ops, SparseCore 1:
  173.1 95.9 all-gather.11
  270.5 17.6 all-gather.5
  290.2 92.1 all-gather.7
  384.6 90.2 all-gather.9
